TPU v7x, 256 devices: a 4x2x16 block of a 4x16x16 slice. The times are simulated.
256 devices in a mesh: grp: 2 (over y), fs: 16 (over z), tp: 8 (over x, core).
Axes of the slice: x: 4, y: 2, z: 16, core: 2. Of those that a mesh axis runs over, the one named last changes fastest.
The devices are a block of a 4x16x16 slice.
Arguments:
- layer_input: bfloat16 [12288, 2048], P(('grp', 'fs'), 'tp'), parts along dimension 0, may hold values from -6 to 6
- first_gain: bfloat16 [1, 2048], P(None, 'tp'), may hold values from 0.099609375 to 1.8984375
- ffn_gate_w: bfloat16 [2048, 6144], P('fs', 'tp'), may hold values from -0.125 to 0.125
- ffn_up_w: bfloat16 [2048, 6144], P('fs', 'tp'), may hold values from -0.125 to 0.125
- ffn_down_w: bfloat16 [6144, 2048], P('tp', 'fs'), may hold values from -0.078125 to 0.078125
- mixer_gain: bfloat16 [1, 2048], P(None, 'tp'), may hold values from 0.099609375 to 1.8984375
- pool_in_w: bfloat16 [2048, 1024], P('fs', 'tp'), may hold values from -0.125 to 0.125
- mixer_gate_w: bfloat16 [2048, 2048], P('fs', 'tp'), may hold values from -0.125 to 0.125
- group_mix_w: bfloat16 [8, 128, 128], P('tp'), may hold values from -0.5 to 0.5
- pool_scale: float32 [1, 1024], P(None, 'tp'), may hold values from 0.1 to 1.9
- mixer_out_w: bfloat16 [1024, 2048], P('tp', 'fs'), may hold values from -0.1875 to 0.1875
- second_gain: bfloat16 [1, 2048], P(None, 'tp'), may hold values from 0.099609375 to 1.8984375
Outputs:
- layer_output: bfloat16 [12288, 2048], P(('grp', 'fs'), 'tp'), parts along dimension 0
There are 2 independent parts, one for each index of `grp`. A program takes and returns all parts, laid end to end along the dimension named above; an argument that names none is the same for every part. Nothing has to cross between parts.
All inputs are finite; a program needn't handle non-finite values.
Results may differ from a plain program's by a relative error of at most 0.015.
Values may be sent and summed in bfloat16 or wider, within the bound.
A program may use at most 64 MiB of HBM per device.

v0:
```python
import jax
import jax.numpy as jnp
from jax import lax
from jax.sharding import Mesh
from jax.sharding import PartitionSpec as P

TP = ("tp_0", "tp_1")


def from_everyone(value, axis):
    length = lax.axis_size(axis)
    return lax.all_to_all(
        jnp.broadcast_to(value[None], (length, *value.shape)), axis, 0, 0, tiled=True
    )


def joined_along(tiles, dim):
    shape = list(tiles.shape[1:])
    shape[dim] *= tiles.shape[0]
    return jnp.moveaxis(tiles, 0, dim).reshape(shape)


def whole_of(value, axes, dim):
    far, near = axes
    initial = from_everyone(value, far)
    tiles = jnp.swapaxes(from_everyone(initial, near), 0, 1)
    return joined_along(tiles.reshape(-1, *value.shape), dim)


def in_one_piece(arrays, axis, dim, along):
    widths = [a.shape[along] for a in arrays]
    both = jnp.concatenate(arrays, axis=along)
    filled = whole_of(both, axis, dim)
    return tuple(jnp.split(filled, [sum(widths[:k]) for k in range(1, len(widths))], axis=along))


def in_blocks(value, dim, length):
    before, after = (value.shape[:dim], value.shape[dim + 1 :])
    return jnp.moveaxis(value.reshape(*before, length, -1, *after), dim, 0)


def summed_on_arrival(value, axis, dim):
    tiles = in_blocks(value, dim, lax.axis_size(axis))
    arrived = lax.all_to_all(tiles, axis, split_axis=0, concat_axis=0, tiled=True)
    return arrived.astype(jnp.float32).sum(axis=0)


def sent_together(arrays, axis, dim, along):
    ends, at = ([], 0)
    for a in arrays[:-1]:
        at += a.shape[along]
        ends.append(at)
    both = jnp.concatenate(arrays, axis=along)
    return tuple(jnp.split(lax.all_gather(both, axis, axis=dim, tiled=True), ends, axis=along))


def gather_directly(value, axis, dim):
    return joined_along(from_everyone(value, axis), dim)


def norm_rows(values, gain):
    gathered, gain_whole = in_one_piece((values, gain), ("tp_0", "tp_1"), 1, 0)
    widened = gathered.astype(jnp.float32)
    scaled = (widened * gain_whole.astype(jnp.float32)).astype(jnp.bfloat16)
    factor = lax.rsqrt(jnp.mean(widened * widened, axis=1, keepdims=True) + 1e-06)
    return (scaled, factor)


def column_sums(partial_value):
    return summed_on_arrival(partial_value.astype(jnp.bfloat16), TP, 1)


def add_pair(scaled, pieces):
    first_sum = jnp.dot(scaled, pieces[0], preferred_element_type=jnp.float32)
    second_sum = jnp.dot(scaled, pieces[1], preferred_element_type=jnp.float32)
    return (first_sum, second_sum)


def per_device(
    layer_input,
    first_gain,
    ffn_gate_w,
    ffn_up_w,
    ffn_down_w,
    mixer_gain,
    pool_in_w,
    mixer_gate_w,
    group_mix_w,
    pool_scale,
    mixer_out_w,
    second_gain,
):
    row_count = layer_input.shape[0]
    gate_whole, up_whole = sent_together((ffn_gate_w, ffn_up_w), "fs", 0, 1)
    down_whole = lax.all_gather(ffn_down_w, "fs", axis=1, tiled=True)

    def feed_forward(values, gain):
        scaled, factor = norm_rows(values, gain)
        gate_pre = factor * jnp.dot(scaled, gate_whole, preferred_element_type=jnp.float32)
        up_pre = factor * jnp.dot(scaled, up_whole, preferred_element_type=jnp.float32)
        hidden = (jax.nn.silu(gate_pre) * up_pre).astype(jnp.bfloat16)
        return jnp.dot(hidden, down_whole, preferred_element_type=jnp.float32)

    first = (
        layer_input.astype(jnp.float32) + 0.5 * column_sums(feed_forward(layer_input, first_gain))
    ).astype(jnp.bfloat16)
    scaled, factor = norm_rows(first, mixer_gain)
    pool_sum, gate_sum = add_pair(scaled, sent_together((pool_in_w, mixer_gate_w), "fs", 0, 1))
    pool_pre = (factor * pool_sum).astype(jnp.bfloat16)
    gate_logit = factor * gate_sum
    group_count = group_mix_w.shape[0]
    group_width = group_mix_w.shape[1]
    first_group = lax.axis_index(TP) * group_count
    values = pool_pre.astype(jnp.float32).reshape(row_count, group_count, group_width)
    running = jnp.cumsum(values, axis=0)
    positions = jnp.arange(row_count, dtype=jnp.int32)
    windows = 2 ** (1 + (first_group + jnp.arange(group_count, dtype=jnp.int32)) % 4)
    chosen = jnp.zeros_like(values)
    for span in (2, 4, 8, 16):
        lagged = jnp.pad(running, ((span, 0), (0, 0), (0, 0)))[:row_count]
        counts = jnp.minimum(positions + 1, span).astype(jnp.float32)[:, None, None]
        means = (running - lagged) / counts
        chosen = jnp.where((windows == span)[None, :, None], means, chosen)
    trail = (chosen - values).astype(jnp.bfloat16)
    mixed = jnp.einsum("tgc,gcd->tgd", trail, group_mix_w, preferred_element_type=jnp.float32)
    pooled = (mixed.reshape(row_count, group_count * group_width) * pool_scale).astype(jnp.bfloat16)
    lifted = column_sums(
        jnp.dot(pooled, gather_directly(mixer_out_w, "fs", 1), preferred_element_type=jnp.float32)
    )
    second = (first.astype(jnp.float32) + jax.nn.sigmoid(gate_logit) * lifted).astype(jnp.bfloat16)
    result = second.astype(jnp.float32) + 0.5 * column_sums(feed_forward(second, second_gain))
    return result.astype(jnp.bfloat16)


def solution(mesh):
    finer = Mesh(
        mesh.devices.reshape(mesh.shape["grp"], mesh.shape["fs"], 4, 2),
        ("grp", "fs", "tp_0", "tp_1"),
    )
    return jax.shard_map(
        per_device,
        mesh=finer,
        in_specs=(
            P(("grp", "fs"), TP),
            P(None, TP),
            P("fs", TP),
            P("fs", TP),
            P(TP, "fs"),
            P(None, TP),
            P("fs", TP),
            P("fs", TP),
            P(TP, None, None),
            P(None, TP),
            P(TP, "fs"),
            P(None, TP),
        ),
        out_specs=P(("grp", "fs"), TP),
        check_vma=False,
    )
```

profile of v0, /device:TPU:33, one launch (start us, length us, event | category | flops | bytes accessed | tf_op | source)
XLA Modules:
  0.0 387.3 jit_solution(81376959434211735)
XLA Ops:
  6.6 1.8 pad_maximum_fusion
  8.5 0.7 all-gather.6.cloned.1.call-update
  9.2 1.0 pad_maximum_fusion.1
  10.3 13.3 %all_to_all.50 = bf16[4,385,256]{2,1,0:T(8,128)(2,1)S(1)} all-to-all(bf16[4,385,256]{2,1,0:T(8,128)(2,1)S(1)} %broadcast_in_dim.91), channel_id=1, replica_groups=mesh['grp'=2,'fs'=16,'tp_0'=4,'tp_1'=2] {'tp_0'}, dimensions={0} | all-to-all | bytes 1576960 | tf_op jit(solution)/shard_map/all_to_all | solution.py:12
  23.6 0.3 copy.33
  23.9 0.4 broadcast_in_dim.92
  24.3 23.7 %all_to_all.51 = bf16[2,4,385,256]{3,1,2,0:T(4,128)(2,1)S(1)} all-to-all(bf16[2,4,385,256]{3,1,2,0:T(4,128)(2,1)S(1)} %broadcast_in_dim.92), channel_id=1, replica_groups=mesh['grp'=2,'fs'=16,'tp_0'=4,'tp_1'=2] {'tp_1'}, dimensions={0} | all-to-all | bytes 3153920 | tf_op jit(solution)/shard_map/all_to_all | solution.py:12
  48.0 0.2 copy.34
  48.2 1.9 slice_convert_fusion.2
  50.2 3.6 copy.35
  53.7 0.4 multiply_reduce_fusion.2
  54.1 2.3 fusion.2
  56.4 48.7 %all-gather.4.cloned.1.call-done = bf16[2048,1536]{1,0:T(8,128)(2,1)} async-done(((bf16[128,1536]{1,0:T(8,128)(2,1)}), bf16[2048,1536]{1,0:T(8,128)(2,1)}) %all-gather.4.cloned.1.call-update) | async-done | bytes 6291472 | tf_op jit(solution)/shard_map/all_gather | solution.py:54
  105.1 4.3 %fusion.11 = f32[384,768]{1,0:T(8,128)} fusion(bf16[384,2048]{0,1:T(8,128)(2,1)S(1)} %fusion.2, bf16[2048,1536]{1,0:T(8,128)(2,1)} %all-gather.4.cloned.1.call-done, f32[384]{0:T(512)S(1)} %add_rsqrt_fusion.2), kind=kOutput, calls=%fused_computation.29 | convolution fusion | flops 1208254464 | bytes 5899776 | tf_op jit(solution)/shard_map/dot_general | solution.py:99
  109.4 71.1 %all-gather.6.cloned.1.call-done = bf16[768,2048]{1,0:T(8,128)(2,1)} async-done(((bf16[768,128]{1,0:T(8,128)(2,1)}), bf16[768,2048]{1,0:T(8,128)(2,1)}) %all-gather.6.cloned.1.call-update) | async-done | bytes 3145744 | tf_op jit(solution)/shard_map/all_gather | solution.py:95
  180.5 6.4 %convolution_convert_fusion.1 = bf16[384,2048]{1,0:T(8,128)(2,1)S(1)} fusion(bf16[768,2048]{1,0:T(8,128)(2,1)} %all-gather.6.cloned.1.call-done, bf16[384,2048]{0,1:T(8,128)(2,1)S(1)} %fusion.2, bf16[2048,1536]{1,0:T(8,128)(2,1)} %all-gather.4.cloned.1.call-done, f32[384,768]{1,0:T(8,128)} %fusion.11, f32[384]{0:T(512)S(1)} %add_rsqrt_fusion.2), kind=kOutput, calls=%fused_computation.13 | convolution fusion | flops 2418769920 | bytes 10618368 | tf_op jit(solution)/shard_map/dot_general | solution.py:102
  186.9 1.3 copy.58
  188.1 15.3 %all-to-all-start.2 = ((bf16[8,384,256]{2,1,0:T(8,128)(2,1)}), bf16[8,384,256]{2,1,0:T(8,128)(2,1)S(1)}, u32[]{:S(2)}, u32[]{:S(2)}) async-start(bf16[8,384,256]{2,1,0:T(8,128)(2,1)} %bitcast.111), calls=%async_computation.2 | async-start | bytes 3145728 | tf_op jit(solution)/shard_map/all_to_all | solution.py:44
  203.5 0.7 pad_maximum_fusion.4
  204.2 19.8 %all-to-all-done.2 = bf16[8,384,256]{2,1,0:T(8,128)(2,1)S(1)} async-done(((bf16[8,384,256]{2,1,0:T(8,128)(2,1)}), bf16[8,384,256]{2,1,0:T(8,128)(2,1)S(1)}, u32[]{:S(2)}, u32[]{:S(2)}) %all-to-all-start.2) | async-done | bytes 1572896 | tf_op jit(solution)/shard_map/all_to_all | solution.py:44
  224.0 0.2 convert_reduce_fusion.2
  224.4 0.9 broadcast_in_dim.93
  225.3 3.6 all-to-all-start.3
  228.9 0.1 copy.42
  229.1 11.3 %all-to-all-done.3 = bf16[4,385,256]{2,1,0:T(8,128)(2,1)S(1)} async-done(((bf16[4,385,256]{2,1,0:T(8,128)(2,1)}), bf16[4,385,256]{2,1,0:T(8,128)(2,1)S(1)}, u32[]{:S(2)}, u32[]{:S(2)}) %all-to-all-start.3) | async-done | bytes 788512 | tf_op jit(solution)/shard_map/all_to_all | solution.py:12
  240.4 0.3 copy.37
  240.7 0.4 broadcast_in_dim.94
  241.1 6.5 %all_to_all.52 = bf16[2,4,385,256]{3,1,2,0:T(4,128)(2,1)S(1)} all-to-all(bf16[2,4,385,256]{3,1,2,0:T(4,128)(2,1)S(1)} %broadcast_in_dim.94), channel_id=1, replica_groups=mesh['grp'=2,'fs'=16,'tp_0'=4,'tp_1'=2] {'tp_1'}, dimensions={0} | all-to-all | bytes 3153920 | tf_op jit(solution)/shard_map/all_to_all | solution.py:12
  247.6 0.9 broadcast_in_dim.104
  248.5 7.0 %all-to-all-start.5 = ((bf16[16,128,128]{1,2,0:T(8,128)(2,1)}), bf16[16,128,128]{1,2,0:T(8,128)(2,1)}, u32[]{:S(2)}, u32[]{:S(2)}) async-start(bf16[16,128,128]{1,2,0:T(8,128)(2,1)} %broadcast_in_dim.104), calls=%async_computation.5 | async-start | bytes 1048576 | tf_op jit(solution)/shard_map/all_to_all | solution.py:12
  255.4 0.2 copy.38
  255.7 1.9 slice_convert_fusion.1
  257.6 3.5 copy.39
  261.1 0.4 multiply_reduce_fusion.1
  261.5 2.2 fusion.1
  263.8 3.6 all-gather.8.cloned.1.call-done
  267.4 1.6 fusion.47
  269.1 0.7 copy-done.6
  269.8 0.1 fusion.58
  270.0 0.7 fusion.73
  270.7 10.8 %all-to-all-done.5 = bf16[16,128,128]{1,2,0:T(8,128)(2,1)} async-done(((bf16[16,128,128]{1,2,0:T(8,128)(2,1)}), bf16[16,128,128]{1,2,0:T(8,128)(2,1)}, u32[]{:S(2)}, u32[]{:S(2)}) %all-to-all-start.5) | async-done | bytes 524320 | tf_op jit(solution)/shard_map/all_to_all | solution.py:12
  281.5 2.4 convolution_convert_fusion.2
  284.0 31.3 %all_to_all.53 = bf16[8,384,256]{2,1,0:T(8,128)(2,1)S(1)} all-to-all(bf16[8,384,256]{2,1,0:T(8,128)(2,1)S(1)} %bitcast.125), channel_id=1, replica_groups=mesh['grp'=2,'fs'=16,'tp_0'=4,'tp_1'=2] {'tp_0','tp_1'}, dimensions={0} | all-to-all | bytes 3145728 | tf_op jit(solution)/shard_map/all_to_all | solution.py:44
  315.3 0.2 convert_reduce_fusion.1
  315.5 1.2 copy-done.12
  316.7 0.7 fusion.41
  317.4 0.6 copy-done.4
  318.1 13.9 %all_to_all.54 = bf16[4,385,256]{2,1,0:T(8,128)(2,1)S(1)} all-to-all(bf16[4,385,256]{2,1,0:T(8,128)(2,1)S(1)} %broadcast_in_dim.105), channel_id=1, replica_groups=mesh['grp'=2,'fs'=16,'tp_0'=4,'tp_1'=2] {'tp_0'}, dimensions={0} | all-to-all | bytes 1576960 | tf_op jit(solution)/shard_map/all_to_all | solution.py:12
  332.0 0.3 copy.44
  332.3 0.4 broadcast_in_dim.106
  332.7 6.5 %all_to_all.55 = bf16[2,4,385,256]{3,1,2,0:T(4,128)(2,1)S(1)} all-to-all(bf16[2,4,385,256]{3,1,2,0:T(4,128)(2,1)S(1)} %broadcast_in_dim.106), channel_id=1, replica_groups=mesh['grp'=2,'fs'=16,'tp_0'=4,'tp_1'=2] {'tp_1'}, dimensions={0} | all-to-all | bytes 3153920 | tf_op jit(solution)/shard_map/all_to_all | solution.py:12
  339.3 0.2 copy.45
  339.5 1.9 slice_convert_fusion
  341.4 0.4 multiply_reduce_fusion
  341.8 2.4 copy.46
  344.2 0.3 fusion
  344.6 1.2 copy-done.2
  345.7 3.3 fusion.14
  349.1 6.5 %convolution_convert_fusion = bf16[384,2048]{1,0:T(8,128)(2,1)S(1)} fusion(bf16[768,2048]{1,0:T(8,128)(2,1)} %all-gather.6.cloned.1.call-done, bf16[384,2048]{0,1:T(8,128)(2,1)} %copy-done.2, bf16[2048,1536]{1,0:T(8,128)(2,1)} %all-gather.4.cloned.1.call-done, f32[384,768]{1,0:T(8,128)S(1)} %fusion.14, f32[384]{0:T(512)S(1)} %add_rsqrt_fusion), kind=kOutput, calls=%fused_computation.12 | convolution fusion | flops 2418769920 | bytes 10618368 | tf_op jit(solution)/shard_map/dot_general | solution.py:102
  355.6 0.1 copy.56
  355.7 23.4 %all_to_all.56 = bf16[8,384,256]{2,1,0:T(8,128)(2,1)S(1)} all-to-all(bf16[8,384,256]{2,1,0:T(8,128)(2,1)S(1)} %bitcast.126), channel_id=1, replica_groups=mesh['grp'=2,'fs'=16,'tp_0'=4,'tp_1'=2] {'tp_0','tp_1'}, dimensions={0} | all-to-all | bytes 3145728 | tf_op jit(solution)/shard_map/all_to_all | solution.py:44
  379.1 0.2 convert_reduce_fusion
  379.3 0.7 copy-done.5
  380.0 0.7 add_convert_fusion
  (47 shorter events, 0.7 us)
Async XLA Ops:
  6.5 275.0 %copy-start = (bf16[1,128,128]{2,1,0:T(8,128)(2,1)S(1)}, bf16[1,128,128]{2,1,0:T(8,128)(2,1)}, u32[]{:S(2)}) copy-start(bf16[1,128,128]{2,1,0:T(8,128)(2,1)} %param.20) | copy-start | bytes 98308
  6.6 98.6 %all-gather.4.cloned.1.call-start = ((), (), s32[]{:S(2)}) async-start(), calls=%async_computation.10 | async-start | bytes 6684672 | tf_op jit(solution)/shard_map/all_gather | solution.py:54
  8.4 172.1 %all-gather.6.cloned.1.call-start = ((), (), s32[]{:S(2)}) async-start(), calls=%async_computation.11 | async-start | bytes 3342336 | tf_op jit(solution)/shard_map/all_gather | solution.py:95
  188.1 15.4 %copy-start.7 = (bf16[128,256]{1,0:T(8,128)(2,1)S(1)}, bf16[128,256]{1,0:T(8,128)(2,1)}, u32[]{:S(2)}) copy-start(bf16[128,256]{1,0:T(8,128)(2,1)} %param.19) | copy-start | bytes 196612
  188.1 15.4 %copy-start.9 = (bf16[128,128]{1,0:T(8,128)(2,1)S(1)}, bf16[128,128]{1,0:T(8,128)(2,1)}, u32[]{:S(2)}) copy-start(bf16[128,128]{1,0:T(8,128)(2,1)} %param.18) | copy-start | bytes 98308
  188.1 35.9 %all-to-all-start.2 = ((bf16[8,384,256]{2,1,0:T(8,128)(2,1)}), bf16[8,384,256]{2,1,0:T(8,128)(2,1)S(1)}, u32[]{:S(2)}, u32[]{:S(2)}) async-start(bf16[8,384,256]{2,1,0:T(8,128)(2,1)} %bitcast.111), calls=%async_computation.2 | async-start | bytes 3145728 | tf_op jit(solution)/shard_map/all_to_all | solution.py:44
  203.4 20.8 %copy-start.3 = (bf16[384,256]{1,0:T(8,128)(2,1)S(1)}, bf16[384,256]{1,0:T(8,128)(2,1)}, u32[]{:S(2)}) copy-start(bf16[384,256]{1,0:T(8,128)(2,1)} %param.12) | copy-start | bytes 589828
  203.4 20.9 %copy-start.10 = (bf16[1,256]{1,0:T(2,128)(2,1)S(1)}, bf16[1,256]{1,0:T(2,128)(2,1)}, u32[]{:S(2)}) copy-start(bf16[1,256]{1,0:T(2,128)(2,1)} %param.17) | copy-start | bytes 1540
  203.4 64.0 %all-gather.8.cloned.1.call-start = ((), (), s32[]{:S(2)}) async-start(), calls=%async_computation.12 | async-start | bytes 1671168 | tf_op jit(solution)/shard_map/all_gather | solution.py:54
  224.3 4.6 %copy-start.8 = (bf16[128,128]{1,0:T(8,128)(2,1)S(1)}, bf16[128,128]{1,0:T(8,128)(2,1)}, u32[]{:S(2)}) copy-start(bf16[128,128]{1,0:T(8,128)(2,1)} %param.22) | copy-start | bytes 98308
  225.3 15.1 %all-to-all-start.3 = ((bf16[4,385,256]{2,1,0:T(8,128)(2,1)}), bf16[4,385,256]{2,1,0:T(8,128)(2,1)S(1)}, u32[]{:S(2)}, u32[]{:S(2)}) async-start(bf16[4,385,256]{2,1,0:T(8,128)(2,1)} %broadcast_in_dim.93), calls=%async_computation.3 | async-start | bytes 1605632 | tf_op jit(solution)/shard_map/all_to_all | solution.py:12
  248.5 33.0 %all-to-all-start.5 = ((bf16[16,128,128]{1,2,0:T(8,128)(2,1)}), bf16[16,128,128]{1,2,0:T(8,128)(2,1)}, u32[]{:S(2)}, u32[]{:S(2)}) async-start(bf16[16,128,128]{1,2,0:T(8,128)(2,1)} %broadcast_in_dim.104), calls=%async_computation.5 | async-start | bytes 1048576 | tf_op jit(solution)/shard_map/all_to_all | solution.py:12
  269.1 0.7 copy-start.6
  269.1 12.4 %copy-start.13 = (f32[1,128]{1,0:T(1,128)S(1)}, f32[1,128]{1,0:T(1,128)}, u32[]{:S(2)}) copy-start(f32[1,128]{1,0:T(1,128)} %param.21) | copy-start | bytes 1540
  315.3 1.4 copy-start.12
  316.7 0.7 copy-start.11
  317.4 0.7 copy-start.4
  344.6 1.2 copy-start.2
  355.7 25.1 %copy-start.1 = (bf16[1,128,128]{2,1,0:T(8,128)(2,1)S(1)}, bf16[1,128,128]{2,1,0:T(8,128)(2,1)}, u32[]{:S(2)}) copy-start(bf16[1,128,128]{2,1,0:T(8,128)(2,1)} %param.20) | copy-start | bytes 98308
  379.1 0.9 copy-start.5
Sparse Core Ops, SparseCore 0:
  9.1 95.9 all-gather.3
  106.8 73.5 all-gather.5
  206.1 61.3 all-gather.7
where the time goes:
time: 388 us; the launch traced here: 387 us
  waiting for transfers between devices  166 us (43%)
  blocking collectives  119 us (31%)
  starting transfers between devices  26 us (7%)
  matrix products  25.2 us (6%)
  local copies, waits for them, and re-layouts  20.2 us (5%)
  other arithmetic  17.6 us (5%)
  between operations  13.6 us (4%)
    all_gather x1, waiting for transfers between devices, per_device(): down_whole = lax.all_gather(ffn_down_w, 'fs', axis=1, tiled=True)  71.1 us
    all_to_all x5, blocking collectives, from_everyone(): lax.all_to_all(jnp.broadcast_to(value[None], (length, *value.shape)), axi...  64 us
    all_to_all x2, blocking collectives, summed_on_arrival(): lax.all_to_all(tiles, axis, split_axis=0, concat_axis=0, tiled=True)  54.7 us
    all_gather x2, waiting for transfers between devices, sent_together(): lax.all_gather(both, axis, axis=dim, tiled=True)  52.3 us
    all_to_all x2, waiting for transfers between devices, from_everyone(): lax.all_to_all(jnp.broadcast_to(value[None], (length, *value.shape)), axi...  22.1 us
    all_to_all x1, waiting for transfers between devices, summed_on_arrival(): lax.all_to_all(tiles, axis, split_axis=0, concat_axis=0, tiled=True)  19.8 us
    all_to_all x1, starting transfers between devices, summed_on_arrival(): lax.all_to_all(tiles, axis, split_axis=0, concat_axis=0, tiled=True)  15.3 us
    dot_general x2, matrix products, feed_forward(): return jnp.dot(hidden, down_whole, preferred_element_type=jnp.float32)  12.9 us
  transfers between devices with their start and end apart: 6, of which 6 were waited for; matrix products, arithmetic and copies ran while one was open for 7% of the time, Pallas kernels for 0%

commit v1 on v0

--- a/solution.py
+++ b/solution.py
@@ -1,3 +1,4 @@
+import functools
 import jax
 import jax.numpy as jnp
 from jax import lax
@@ -5,6 +6,41 @@
 from jax.sharding import PartitionSpec as P
 
 TP = ("tp_0", "tp_1")
+
+
+def stacks_all_obtain(row_data, k_dim):
+    b_now = list(row_data.shape[1:])
+    b_now[k_dim] *= row_data.shape[0]
+    local_part = jnp.moveaxis(row_data, 0, k_dim).reshape(b_now)
+    return local_part
+
+
+def expand_slot(xs, peer_axis, in_dim):
+    total_devices = lax.psum(1, peer_axis)
+    taken_in = range(total_devices)
+    main = map(lambda to_i: (to_i, (to_i + 1) % total_devices), taken_in)
+    history = list(main)
+    z_new, outer = ([], [])
+    c = 0
+    copies = [(idx, dev_i) for dev_i, idx in history]
+    while c < total_devices - 1:
+        if c % 2 == 0:
+            seen_now = lax.ppermute(z_new[-1] if z_new else xs, perm=history, axis_name=peer_axis)
+            z_new.append(seen_now)
+        else:
+            mid_arr = lax.ppermute(outer[-1] if outer else xs, axis_name=peer_axis, perm=copies)
+            outer.append(mid_arr)
+        c = c + 1
+    u_next = jnp.stack([*z_new[::-1], xs, *outer])
+    block_now = len(z_new)
+    passed = lax.axis_index(peer_axis)
+    b_next = passed - block_now
+    u_next = u_next[(jnp.arange(total_devices) - b_next) % total_devices]
+    right_arr = stacks_all_obtain(u_next, in_dim)
+    return right_arr
+
+
+knots_run = functools.partial(expand_slot, peer_axis="fs", in_dim=1)
 
 
 def from_everyone(value, axis):
@@ -92,7 +128,7 @@
 ):
     row_count = layer_input.shape[0]
     gate_whole, up_whole = sent_together((ffn_gate_w, ffn_up_w), "fs", 0, 1)
-    down_whole = lax.all_gather(ffn_down_w, "fs", axis=1, tiled=True)
+    down_whole = knots_run(ffn_down_w)
 
     def feed_forward(values, gain):
         scaled, factor = norm_rows(values, gain)

time: 388 us -> 348 us (0.90)
  waiting for transfers between devices: 166 us -> 97.6 us
  starting transfers between devices: 26 us -> 58.7 us
  blocking collectives: 119 us -> 91.1 us
  local copies, waits for them, and re-layouts: 20.2 us -> 39.1 us
    all_gather x1 -> x0, waiting for transfers between devices: 71.1 us -> none  [per_device(): down_whole = lax.all_gather(ffn_down_w, 'fs', axis=1, tiled=True)]
    ppermute x0 -> x15, waiting for transfers between devices: none -> 52.1 us  [the longest x8 50 us: expand_slot(): lax.ppermute(z_new[-1] if z_new else xs, perm=history, axis_name=peer_axis)]
    all_gather x2, waiting for transfers between devices: 52.3 us -> 3.18 us  [sent_together(): lax.all_gather(both, axis, axis=dim, tiled=True)]
    ppermute x0 -> x15, starting transfers between devices: none -> 38.1 us  [the longest x7 33.8 us: expand_slot(): lax.ppermute(outer[-1] if outer else xs, axis_name=peer_axis, perm=copies)]
    all_to_all x5 -> x4, blocking collectives: 64 us -> 36.9 us  [from_everyone(): lax.all_to_all(jnp.broadcast_to(value[None], (length, *value.shape)), axi...]
    unnamed x29 -> x48, local copies, waits for them, and re-layouts: 4.51 us -> 13 us
    all_to_all x1, starting transfers between devices: 15.3 us -> 7.86 us  [summed_on_arrival(): lax.all_to_all(tiles, axis, split_axis=0, concat_axis=0, tiled=True)]
    all_to_all x2 -> x3, starting transfers between devices: 10.5 us -> 12.7 us  [from_everyone(): lax.all_to_all(jnp.broadcast_to(value[None], (length, *value.shape)), axi...]
  transfers between devices with their start and end apart: 6 -> 21, of which waited for: 6 -> 12; matrix products, arithmetic and copies ran while one was open for 7% -> 13% of each run, Pallas kernels for 0% -> 0%
where the time goes in v1:
time: 348 us; the launch traced here: 347 us
  waiting for transfers between devices  97.6 us (28%)
  blocking collectives  91.1 us (26%)
  starting transfers between devices  58.7 us (17%)
  local copies, waits for them, and re-layouts  39.1 us (11%)
  matrix products  28.2 us (8%)
  other arithmetic  18.8 us (5%)
  between operations  13.9 us (4%)
    all_to_all x2, blocking collectives, summed_on_arrival(): lax.all_to_all(tiles, axis, split_axis=0, concat_axis=0, tiled=True)  54.2 us
    ppermute x8, waiting for transfers between devices, expand_slot(): lax.ppermute(z_new[-1] if z_new else xs, perm=history, axis_name=peer_axis)  50 us
    all_to_all x4, blocking collectives, from_everyone(): lax.all_to_all(jnp.broadcast_to(value[None], (length, *value.shape)), axi...  36.9 us
    ppermute x7, starting transfers between devices, expand_slot(): lax.ppermute(outer[-1] if outer else xs, axis_name=peer_axis, perm=copies)  33.8 us
    all_to_all x3, waiting for transfers between devices, from_everyone(): lax.all_to_all(jnp.broadcast_to(value[None], (length, *value.shape)), axi...  22.4 us
    all_to_all x1, waiting for transfers between devices, summed_on_arrival(): lax.all_to_all(tiles, axis, split_axis=0, concat_axis=0, tiled=True)  19.8 us
    dot_general x2, matrix products, feed_forward(): return jnp.dot(hidden, down_whole, preferred_element_type=jnp.float32)  14 us
    unnamed x48, local copies, waits for them, and re-layouts  13 us
  transfers between devices with their start and end apart: 21, of which 12 were waited for; matrix products, arithmetic and copies ran while one was open for 13% of the time, Pallas kernels for 0%

profile of v1, /device:TPU:33, one launch (start us, length us, event | category | flops | bytes accessed | tf_op | source)
XLA Modules:
  0.0 347.4 jit_solution(13590517608033294383)
XLA Ops:
  6.6 1.8 pad_maximum_fusion
  8.4 3.4 collective-permute-start
  11.9 19.7 %collective-permute-start.8 = (bf16[768,128]{1,0:T(8,128)(2,1)}, bf16[768,128]{1,0:T(8,128)(2,1)S(1)}, u32[]{:S(2)}, u32[]{:S(2)}) collective-permute-start(bf16[768,128]{1,0:T(8,128)(2,1)} %param.16), channel_id=1, source_target_pairs={{8,0},{16,8},{24,16},{32,24},{40,32},{48,40},{56,48},{64,56},{72,6... | collective-permute-start | bytes 589832 | tf_op jit(solution)/shard_map/ppermute | solution.py:31
  31.6 1.0 pad_maximum_fusion.1
  32.6 1.0 broadcast_in_dim.92
  33.5 4.3 %all-to-all-start = ((bf16[4,385,256]{2,1,0:T(8,128)(2,1)}), bf16[4,385,256]{2,1,0:T(8,128)(2,1)S(1)}, u32[]{:S(2)}, u32[]{:S(2)}) async-start(bf16[4,385,256]{2,1,0:T(8,128)(2,1)} %broadcast_in_dim.92), calls=%async_computation | async-start | bytes 1605632 | tf_op jit(solution)/shard_map/all_to_all | solution.py:48
  37.9 2.7 collective-permute-start.9
  40.5 6.2 %collective-permute-done.1 = bf16[768,128]{1,0:T(8,128)(2,1)S(1)} collective-permute-done((bf16[768,128]{1,0:T(8,128)(2,1)S(1)}, bf16[768,128]{1,0:T(8,128)(2,1)S(1)}, u32[]{:S(2)}, u32[]{:S(2)}) %collective-permute-start.1) | collective-permute-done | bytes 196640 | tf_op jit(solution)/shard_map/ppermute | solution.py:28
  46.7 0.8 collective-permute-start.2
  47.5 0.9 collective-permute-done.9
  48.5 1.2 collective-permute-start.10
  49.6 8.2 %collective-permute-done.2 = bf16[768,128]{1,0:T(8,128)(2,1)S(1)} collective-permute-done((bf16[768,128]{1,0:T(8,128)(2,1)S(1)}, bf16[768,128]{1,0:T(8,128)(2,1)S(1)}, u32[]{:S(2)}, u32[]{:S(2)}) %collective-permute-start.2) | collective-permute-done | bytes 196640 | tf_op jit(solution)/shard_map/ppermute | solution.py:28
  57.8 1.1 collective-permute-done.10
  59.0 1.5 collective-permute-start.11
  61.2 9.9 %all_to_all.50 = bf16[2,4,385,256]{3,1,2,0:T(4,128)(2,1)S(1)} all-to-all(bf16[2,4,385,256]{3,1,2,0:T(4,128)(2,1)S(1)} %broadcast_in_dim.93), channel_id=1, replica_groups=mesh['grp'=2,'fs'=16,'tp_0'=4,'tp_1'=2] {'tp_1'}, dimensions={0} | all-to-all | bytes 3153920 | tf_op jit(solution)/shard_map/all_to_all | solution.py:48
  71.4 1.9 slice_convert_fusion.2
  73.3 3.7 %copy.43 = f32[384,8,256]{0,2,1:T(8,128)} copy(f32[384,8,256]{2,0,1:T(8,128)} %slice_convert_fusion.2) | data formatting | bytes 6291456 | tf_op jit(solution)/shard_map/convert_element_type | solution.py:99
  77.0 12.3 %collective-permute-done.4 = bf16[768,128]{1,0:T(8,128)(2,1)S(1)} collective-permute-done((bf16[768,128]{1,0:T(8,128)(2,1)S(1)}, bf16[768,128]{1,0:T(8,128)(2,1)S(1)}, u32[]{:S(2)}, u32[]{:S(2)}) %collective-permute-start.4) | collective-permute-done | bytes 196640 | tf_op jit(solution)/shard_map/ppermute | solution.py:28
  89.4 3.4 fusion.2
  92.7 2.7 collective-permute-start.12
  95.4 6.1 %collective-permute-done.5 = bf16[768,128]{1,0:T(8,128)(2,1)S(1)} collective-permute-done((bf16[768,128]{1,0:T(8,128)(2,1)S(1)}, bf16[768,128]{1,0:T(8,128)(2,1)S(1)}, u32[]{:S(2)}, u32[]{:S(2)}) %collective-permute-start.5) | collective-permute-done | bytes 196640 | tf_op jit(solution)/shard_map/ppermute | solution.py:28
  101.9 3.1 collective-permute-start.13
  105.0 8.4 %collective-permute-done.6 = bf16[768,128]{1,0:T(8,128)(2,1)S(1)} collective-permute-done((bf16[768,128]{1,0:T(8,128)(2,1)S(1)}, bf16[768,128]{1,0:T(8,128)(2,1)S(1)}, u32[]{:S(2)}, u32[]{:S(2)}) %collective-permute-start.6) | collective-permute-done | bytes 196640 | tf_op jit(solution)/shard_map/ppermute | solution.py:28
  113.4 2.9 collective-permute-start.14
  116.3 8.8 %collective-permute-done.7 = bf16[768,128]{1,0:T(8,128)(2,1)S(1)} collective-permute-done((bf16[768,128]{1,0:T(8,128)(2,1)S(1)}, bf16[768,128]{1,0:T(8,128)(2,1)S(1)}, u32[]{:S(2)}, u32[]{:S(2)}) %collective-permute-start.7) | collective-permute-done | bytes 196640 | tf_op jit(solution)/shard_map/ppermute | solution.py:28
  125.8 0.7 bitcast_dynamic-update-slice_fusion.14
  127.2 0.7 bitcast_dynamic-update-slice_fusion.12
  130.6 0.7 bitcast_dynamic-update-slice_fusion.7
  132.1 0.7 bitcast_dynamic-update-slice_fusion.5
  132.8 0.7 bitcast_dynamic-update-slice_fusion.4
  133.5 0.7 bitcast_dynamic-update-slice_fusion.3
  134.2 0.7 bitcast_dynamic-update-slice_fusion.2
  134.9 0.7 bitcast_dynamic-update-slice_fusion.1
  136.3 3.0 gather_fusion
  139.3 2.9 copy.44
  142.2 5.0 %fusion.11 = f32[384,768]{1,0:T(8,128)} fusion(bf16[384,2048]{0,1:T(8,128)(2,1)} %fusion.2, bf16[2048,1536]{1,0:T(8,128)(2,1)} %all-gather.3.cloned.1.call-done, f32[384]{0:T(512)S(1)} %add_rsqrt_fusion.2), kind=kOutput, calls=%fused_computation.30 | convolution fusion | flops 1208254464 | bytes 5899776 | tf_op jit(solution)/shard_map/dot_general | solution.py:135
  147.2 7.0 %convolution_convert_fusion.1 = bf16[384,2048]{1,0:T(8,128)(2,1)} fusion(bf16[768,2048]{0,1:T(8,128)(2,1)S(1)} %bitcast.164, bf16[384,2048]{0,1:T(8,128)(2,1)} %fusion.2, bf16[2048,1536]{1,0:T(8,128)(2,1)} %all-gather.3.cloned.1.call-done, f32[384,768]{1,0:T(8,128)} %fusion.11, f32[384]{0:T(512)S(1)} %add_rsqrt_fusion.2), kind=kOutput, calls=%fused_computation.14 | convolution fusion | flops 2418769920 | bytes 10618368 | tf_op jit(solution)/shard_map/dot_general | solution.py:138
  154.2 2.7 copy.67
  156.9 7.9 %all-to-all-start.2 = ((bf16[8,384,256]{2,1,0:T(8,128)(2,1)}), bf16[8,384,256]{2,1,0:T(8,128)(2,1)S(1)}, u32[]{:S(2)}, u32[]{:S(2)}) async-start(bf16[8,384,256]{2,1,0:T(8,128)(2,1)} %bitcast.147), calls=%async_computation.2 | async-start | bytes 3145728 | tf_op jit(solution)/shard_map/all_to_all | solution.py:80
  165.5 19.8 %all-to-all-done.2 = bf16[8,384,256]{2,1,0:T(8,128)(2,1)S(1)} async-done(((bf16[8,384,256]{2,1,0:T(8,128)(2,1)}), bf16[8,384,256]{2,1,0:T(8,128)(2,1)S(1)}, u32[]{:S(2)}, u32[]{:S(2)}) %all-to-all-start.2) | async-done | bytes 1572896 | tf_op jit(solution)/shard_map/all_to_all | solution.py:80
  185.6 0.9 broadcast_in_dim.94
  186.6 3.6 %all-to-all-start.3 = ((bf16[4,385,256]{2,1,0:T(8,128)(2,1)}), bf16[4,385,256]{2,1,0:T(8,128)(2,1)S(1)}, u32[]{:S(2)}, u32[]{:S(2)}) async-start(bf16[4,385,256]{2,1,0:T(8,128)(2,1)} %broadcast_in_dim.94), calls=%async_computation.3 | async-start | bytes 1605632 | tf_op jit(solution)/shard_map/all_to_all | solution.py:48
  190.3 11.3 %all-to-all-done.3 = bf16[4,385,256]{2,1,0:T(8,128)(2,1)S(1)} async-done(((bf16[4,385,256]{2,1,0:T(8,128)(2,1)}), bf16[4,385,256]{2,1,0:T(8,128)(2,1)S(1)}, u32[]{:S(2)}, u32[]{:S(2)}) %all-to-all-start.3) | async-done | bytes 788512 | tf_op jit(solution)/shard_map/all_to_all | solution.py:48
  202.4 6.5 %all_to_all.51 = bf16[2,4,385,256]{3,1,2,0:T(4,128)(2,1)S(1)} all-to-all(bf16[2,4,385,256]{3,1,2,0:T(4,128)(2,1)S(1)} %broadcast_in_dim.95), channel_id=1, replica_groups=mesh['grp'=2,'fs'=16,'tp_0'=4,'tp_1'=2] {'tp_1'}, dimensions={0} | all-to-all | bytes 3153920 | tf_op jit(solution)/shard_map/all_to_all | solution.py:48
  208.8 0.9 broadcast_in_dim.105
  209.7 4.8 %all-to-all-start.5 = ((bf16[16,128,128]{1,2,0:T(8,128)(2,1)}), bf16[16,128,128]{1,2,0:T(8,128)(2,1)}, u32[]{:S(2)}, u32[]{:S(2)}) async-start(bf16[16,128,128]{1,2,0:T(8,128)(2,1)} %broadcast_in_dim.105), calls=%async_computation.5 | async-start | bytes 1048576 | tf_op jit(solution)/shard_map/all_to_all | solution.py:48
  214.8 1.9 slice_convert_fusion.1
  216.8 3.5 %copy.48 = f32[384,8,256]{0,2,1:T(8,128)} copy(f32[384,8,256]{2,0,1:T(8,128)} %slice_convert_fusion.1) | data formatting | bytes 6291456 | tf_op jit(solution)/shard_map/convert_element_type | solution.py:99
  220.7 2.2 fusion.1
  223.0 3.2 all-gather.5.cloned.1.call-done
  226.1 1.6 fusion.47
  229.4 11.1 %all-to-all-done.5 = bf16[16,128,128]{1,2,0:T(8,128)(2,1)} async-done(((bf16[16,128,128]{1,2,0:T(8,128)(2,1)}), bf16[16,128,128]{1,2,0:T(8,128)(2,1)}, u32[]{:S(2)}, u32[]{:S(2)}) %all-to-all-start.5) | async-done | bytes 524320 | tf_op jit(solution)/shard_map/all_to_all | solution.py:48
  240.5 2.4 convolution_convert_fusion.2
  243.0 30.7 %all_to_all.52 = bf16[8,384,256]{2,1,0:T(8,128)(2,1)S(1)} all-to-all(bf16[8,384,256]{2,1,0:T(8,128)(2,1)S(1)} %bitcast.162), channel_id=1, replica_groups=mesh['grp'=2,'fs'=16,'tp_0'=4,'tp_1'=2] {'tp_0','tp_1'}, dimensions={0} | all-to-all | bytes 3145728 | tf_op jit(solution)/shard_map/all_to_all | solution.py:80
  275.4 13.9 %all_to_all.53 = bf16[4,385,256]{2,1,0:T(8,128)(2,1)S(1)} all-to-all(bf16[4,385,256]{2,1,0:T(8,128)(2,1)S(1)} %broadcast_in_dim.106), channel_id=1, replica_groups=mesh['grp'=2,'fs'=16,'tp_0'=4,'tp_1'=2] {'tp_0'}, dimensions={0} | all-to-all | bytes 1576960 | tf_op jit(solution)/shard_map/all_to_all | solution.py:48
  290.0 6.5 %all_to_all.54 = bf16[2,4,385,256]{3,1,2,0:T(4,128)(2,1)S(1)} all-to-all(bf16[2,4,385,256]{3,1,2,0:T(4,128)(2,1)S(1)} %broadcast_in_dim.107), channel_id=1, replica_groups=mesh['grp'=2,'fs'=16,'tp_0'=4,'tp_1'=2] {'tp_1'}, dimensions={0} | all-to-all | bytes 3153920 | tf_op jit(solution)/shard_map/all_to_all | solution.py:48
  296.8 1.9 slice_convert_fusion
  299.1 2.4 copy.55
  301.9 1.1 copy-done.3
  303.0 4.5 %fusion.14 = f32[384,768]{1,0:T(8,128)} fusion(bf16[384,2048]{0,1:T(8,128)(2,1)S(1)} %fusion, bf16[2048,1536]{1,0:T(8,128)(2,1)} %all-gather.3.cloned.1.call-done, f32[384]{0:T(512)S(1)} %add_rsqrt_fusion), kind=kOutput, calls=%fused_computation.31 | convolution fusion | flops 1208254464 | bytes 5899776 | tf_op jit(solution)/shard_map/dot_general | solution.py:135
  307.5 7.0 %convolution_convert_fusion = bf16[384,2048]{1,0:T(8,128)(2,1)} fusion(bf16[768,2048]{0,1:T(8,128)(2,1)S(1)} %bitcast.165, bf16[384,2048]{0,1:T(8,128)(2,1)} %copy-done.3, bf16[2048,1536]{1,0:T(8,128)(2,1)} %all-gather.3.cloned.1.call-done, f32[384,768]{1,0:T(8,128)} %fusion.14, f32[384]{0:T(512)S(1)} %add_rsqrt_fusion), kind=kOutput, calls=%fused_computation.13 | convolution fusion | flops 2418769920 | bytes 10618368 | tf_op jit(solution)/shard_map/dot_general | solution.py:138
  314.5 1.5 copy.65
  316.0 23.6 %all_to_all.55 = bf16[8,384,256]{2,1,0:T(8,128)(2,1)S(1)} all-to-all(bf16[8,384,256]{2,1,0:T(8,128)(2,1)S(1)} %bitcast.163), channel_id=1, replica_groups=mesh['grp'=2,'fs'=16,'tp_0'=4,'tp_1'=2] {'tp_0','tp_1'}, dimensions={0} | all-to-all | bytes 3145728 | tf_op jit(solution)/shard_map/all_to_all | solution.py:80
  339.8 0.7 add_convert_fusion
  (99 shorter events, 14.6 us)
Async XLA Ops:
  6.5 234.0 %copy-start = (bf16[1,128,128]{2,1,0:T(8,128)(2,1)S(1)}, bf16[1,128,128]{2,1,0:T(8,128)(2,1)}, u32[]{:S(2)}) copy-start(bf16[1,128,128]{2,1,0:T(8,128)(2,1)} %param.20) | copy-start | bytes 98308
  6.6 135.6 %all-gather.3.cloned.1.call-start = ((), (), s32[]{:S(2)}) async-start(), calls=%async_computation.10 | async-start | bytes 6684672 | tf_op jit(solution)/shard_map/all_gather | solution.py:90
  8.4 29.4 %collective-permute-start = (bf16[768,128]{1,0:T(8,128)(2,1)}, bf16[768,128]{1,0:T(8,128)(2,1)S(1)}, u32[]{:S(2)}, u32[]{:S(2)}) collective-permute-start(bf16[768,128]{1,0:T(8,128)(2,1)} %param.16), channel_id=1, source_target_pairs={{0,8},{8,16},{16,24},{24,32},{32,40},{40,48},{48,56},{56,64},{64,7... | collective-permute-start | bytes 589832 | tf_op jit(solution)/shard_map/ppermute | solution.py:28
  11.9 26.0 %collective-permute-start.8 = (bf16[768,128]{1,0:T(8,128)(2,1)}, bf16[768,128]{1,0:T(8,128)(2,1)S(1)}, u32[]{:S(2)}, u32[]{:S(2)}) collective-permute-start(bf16[768,128]{1,0:T(8,128)(2,1)} %param.16), channel_id=1, source_target_pairs={{8,0},{16,8},{24,16},{32,24},{40,32},{48,40},{56,48},{64,56},{72,6... | collective-permute-start | bytes 589832 | tf_op jit(solution)/shard_map/ppermute | solution.py:31
  33.5 27.0 %all-to-all-start = ((bf16[4,385,256]{2,1,0:T(8,128)(2,1)}), bf16[4,385,256]{2,1,0:T(8,128)(2,1)S(1)}, u32[]{:S(2)}, u32[]{:S(2)}) async-start(bf16[4,385,256]{2,1,0:T(8,128)(2,1)} %broadcast_in_dim.92), calls=%async_computation | async-start | bytes 1605632 | tf_op jit(solution)/shard_map/all_to_all | solution.py:48
  37.8 8.9 %collective-permute-start.1 = (bf16[768,128]{1,0:T(8,128)(2,1)S(1)}, bf16[768,128]{1,0:T(8,128)(2,1)S(1)}, u32[]{:S(2)}, u32[]{:S(2)}) collective-permute-start(bf16[768,128]{1,0:T(8,128)(2,1)S(1)} %collective-permute-done), channel_id=1, source_target_pairs={{0,8},{8,16},{16,24},{24,32},{32,40},{40,48},{48,56},{56,64},{64,7... | collective-permute-start | bytes 589832 | tf_op jit(solution)/shard_map/ppermute | solution.py:28
  37.9 10.6 %collective-permute-start.9 = (bf16[768,128]{1,0:T(8,128)(2,1)S(1)}, bf16[768,128]{1,0:T(8,128)(2,1)S(1)}, u32[]{:S(2)}, u32[]{:S(2)}) collective-permute-start(bf16[768,128]{1,0:T(8,128)(2,1)S(1)} %collective-permute-done.8), channel_id=1, source_target_pairs={{8,0},{16,8},{24,16},{32,24},{40,32},{48,40},{56,48},{64,56},{72,6... | collective-permute-start | bytes 589832 | tf_op jit(solution)/shard_map/ppermute | solution.py:31
  46.7 11.1 %collective-permute-start.2 = (bf16[768,128]{1,0:T(8,128)(2,1)S(1)}, bf16[768,128]{1,0:T(8,128)(2,1)S(1)}, u32[]{:S(2)}, u32[]{:S(2)}) collective-permute-start(bf16[768,128]{1,0:T(8,128)(2,1)S(1)} %collective-permute-done.1), channel_id=1, source_target_pairs={{0,8},{8,16},{16,24},{24,32},{32,40},{40,48},{48,56},{56,64},{64,7... | collective-permute-start | bytes 589832 | tf_op jit(solution)/shard_map/ppermute | solution.py:28
  48.5 10.5 %collective-permute-start.10 = (bf16[768,128]{1,0:T(8,128)(2,1)S(1)}, bf16[768,128]{1,0:T(8,128)(2,1)S(1)}, u32[]{:S(2)}, u32[]{:S(2)}) collective-permute-start(bf16[768,128]{1,0:T(8,128)(2,1)S(1)} %collective-permute-done.9), channel_id=1, source_target_pairs={{8,0},{16,8},{24,16},{32,24},{40,32},{48,40},{56,48},{64,56},{72,6... | collective-permute-start | bytes 589832 | tf_op jit(solution)/shard_map/ppermute | solution.py:31
  57.8 19.2 %collective-permute-start.3 = (bf16[768,128]{1,0:T(8,128)(2,1)S(1)}, bf16[768,128]{1,0:T(8,128)(2,1)S(1)}, u32[]{:S(2)}, u32[]{:S(2)}) collective-permute-start(bf16[768,128]{1,0:T(8,128)(2,1)S(1)} %collective-permute-done.2), channel_id=1, source_target_pairs={{0,8},{8,16},{16,24},{24,32},{32,40},{40,48},{48,56},{56,64},{64,7... | collective-permute-start | bytes 589832 | tf_op jit(solution)/shard_map/ppermute | solution.py:28
  59.0 33.8 %collective-permute-start.11 = (bf16[768,128]{1,0:T(8,128)(2,1)S(1)}, bf16[768,128]{1,0:T(8,128)(2,1)S(1)}, u32[]{:S(2)}, u32[]{:S(2)}) collective-permute-start(bf16[768,128]{1,0:T(8,128)(2,1)S(1)} %collective-permute-done.10), channel_id=1, source_target_pairs={{8,0},{16,8},{24,16},{32,24},{40,32},{48,40},{56,48},{64,56},{72,6... | collective-permute-start | bytes 589832 | tf_op jit(solution)/shard_map/ppermute | solution.py:31
  77.0 12.3 %collective-permute-start.4 = (bf16[768,128]{1,0:T(8,128)(2,1)S(1)}, bf16[768,128]{1,0:T(8,128)(2,1)S(1)}, u32[]{:S(2)}, u32[]{:S(2)}) collective-permute-start(bf16[768,128]{1,0:T(8,128)(2,1)S(1)} %collective-permute-done.3), channel_id=1, source_target_pairs={{0,8},{8,16},{16,24},{24,32},{32,40},{40,48},{48,56},{56,64},{64,7... | collective-permute-start | bytes 589832 | tf_op jit(solution)/shard_map/ppermute | solution.py:28
  89.4 12.1 %collective-permute-start.5 = (bf16[768,128]{1,0:T(8,128)(2,1)S(1)}, bf16[768,128]{1,0:T(8,128)(2,1)S(1)}, u32[]{:S(2)}, u32[]{:S(2)}) collective-permute-start(bf16[768,128]{1,0:T(8,128)(2,1)S(1)} %collective-permute-done.4), channel_id=1, source_target_pairs={{0,8},{8,16},{16,24},{24,32},{32,40},{40,48},{48,56},{56,64},{64,7... | collective-permute-start | bytes 589832 | tf_op jit(solution)/shard_map/ppermute | solution.py:28
  92.7 37.9 %copy-start.8 = (bf16[768,128]{1,0:T(8,128)(2,1)S(1)}, bf16[768,128]{1,0:T(8,128)(2,1)}, u32[]{:S(2)}) copy-start(bf16[768,128]{1,0:T(8,128)(2,1)} %param.16) | copy-start | bytes 589828
  92.7 9.2 %collective-permute-start.12 = (bf16[768,128]{1,0:T(8,128)(2,1)S(1)}, bf16[768,128]{1,0:T(8,128)(2,1)S(1)}, u32[]{:S(2)}, u32[]{:S(2)}) collective-permute-start(bf16[768,128]{1,0:T(8,128)(2,1)S(1)} %collective-permute-done.11), channel_id=1, source_target_pairs={{8,0},{16,8},{24,16},{32,24},{40,32},{48,40},{56,48},{64,56},{72,6... | collective-permute-start | bytes 589832 | tf_op jit(solution)/shard_map/ppermute | solution.py:31
  101.5 11.9 %collective-permute-start.6 = (bf16[768,128]{1,0:T(8,128)(2,1)S(1)}, bf16[768,128]{1,0:T(8,128)(2,1)S(1)}, u32[]{:S(2)}, u32[]{:S(2)}) collective-permute-start(bf16[768,128]{1,0:T(8,128)(2,1)S(1)} %collective-permute-done.5), channel_id=1, source_target_pairs={{0,8},{8,16},{16,24},{24,32},{32,40},{40,48},{48,56},{56,64},{64,7... | collective-permute-start | bytes 589832 | tf_op jit(solution)/shard_map/ppermute | solution.py:28
  101.9 11.5 %collective-permute-start.13 = (bf16[768,128]{1,0:T(8,128)(2,1)S(1)}, bf16[768,128]{1,0:T(8,128)(2,1)S(1)}, u32[]{:S(2)}, u32[]{:S(2)}) collective-permute-start(bf16[768,128]{1,0:T(8,128)(2,1)S(1)} %collective-permute-done.12), channel_id=1, source_target_pairs={{8,0},{16,8},{24,16},{32,24},{40,32},{48,40},{56,48},{64,56},{72,6... | collective-permute-start | bytes 589832 | tf_op jit(solution)/shard_map/ppermute | solution.py:31
  113.4 11.7 %collective-permute-start.7 = (bf16[768,128]{1,0:T(8,128)(2,1)S(1)}, bf16[768,128]{1,0:T(8,128)(2,1)S(1)}, u32[]{:S(2)}, u32[]{:S(2)}) collective-permute-start(bf16[768,128]{1,0:T(8,128)(2,1)S(1)} %collective-permute-done.6), channel_id=1, source_target_pairs={{0,8},{8,16},{16,24},{24,32},{32,40},{40,48},{48,56},{56,64},{64,7... | collective-permute-start | bytes 589832 | tf_op jit(solution)/shard_map/ppermute | solution.py:28
  113.4 22.1 %collective-permute-start.14 = (bf16[768,128]{1,0:T(8,128)(2,1)S(1)}, bf16[768,128]{1,0:T(8,128)(2,1)S(1)}, u32[]{:S(2)}, u32[]{:S(2)}) collective-permute-start(bf16[768,128]{1,0:T(8,128)(2,1)S(1)} %collective-permute-done.13), channel_id=1, source_target_pairs={{8,0},{16,8},{24,16},{32,24},{40,32},{48,40},{56,48},{64,56},{72,6... | collective-permute-start | bytes 589832 | tf_op jit(solution)/shard_map/ppermute | solution.py:31
  142.2 5.0 %copy-start.1 = (bf16[768,16,128]{0,2,1:T(8,128)(2,1)S(1)}, bf16[768,16,128]{0,2,1:T(8,128)(2,1)}, u32[]{:S(2)}) copy-start(bf16[768,16,128]{0,2,1:T(8,128)(2,1)} %copy.44) | copy-start | bytes 9437188
  154.2 10.6 %copy-start.9 = (bf16[128,256]{1,0:T(8,128)(2,1)S(1)}, bf16[128,256]{1,0:T(8,128)(2,1)}, u32[]{:S(2)}) copy-start(bf16[128,256]{1,0:T(8,128)(2,1)} %param.19) | copy-start | bytes 196612
  154.2 10.6 %copy-start.11 = (bf16[128,128]{1,0:T(8,128)(2,1)S(1)}, bf16[128,128]{1,0:T(8,128)(2,1)}, u32[]{:S(2)}) copy-start(bf16[128,128]{1,0:T(8,128)(2,1)} %param.18) | copy-start | bytes 98308
  156.9 28.7 %copy-start.4 = (bf16[384,256]{1,0:T(8,128)(2,1)S(1)}, bf16[384,256]{1,0:T(8,128)(2,1)}, u32[]{:S(2)}) copy-start(bf16[384,256]{1,0:T(8,128)(2,1)} %param.12) | copy-start | bytes 589828
  156.9 28.7 %copy-start.12 = (bf16[1,256]{1,0:T(2,128)(2,1)S(1)}, bf16[1,256]{1,0:T(2,128)(2,1)}, u32[]{:S(2)}) copy-start(bf16[1,256]{1,0:T(2,128)(2,1)} %param.17) | copy-start | bytes 1540
  156.9 28.4 %all-to-all-start.2 = ((bf16[8,384,256]{2,1,0:T(8,128)(2,1)}), bf16[8,384,256]{2,1,0:T(8,128)(2,1)S(1)}, u32[]{:S(2)}, u32[]{:S(2)}) async-start(bf16[8,384,256]{2,1,0:T(8,128)(2,1)} %bitcast.147), calls=%async_computation.2 | async-start | bytes 3145728 | tf_op jit(solution)/shard_map/all_to_all | solution.py:80
  164.7 25.5 %copy-start.10 = (bf16[128,128]{1,0:T(8,128)(2,1)S(1)}, bf16[128,128]{1,0:T(8,128)(2,1)}, u32[]{:S(2)}) copy-start(bf16[128,128]{1,0:T(8,128)(2,1)} %param.22) | copy-start | bytes 98308
  164.7 61.4 %all-gather.5.cloned.1.call-start = ((), (), s32[]{:S(2)}) async-start(), calls=%async_computation.11 | async-start | bytes 1671168 | tf_op jit(solution)/shard_map/all_gather | solution.py:90
  186.6 15.1 %all-to-all-start.3 = ((bf16[4,385,256]{2,1,0:T(8,128)(2,1)}), bf16[4,385,256]{2,1,0:T(8,128)(2,1)S(1)}, u32[]{:S(2)}, u32[]{:S(2)}) async-start(bf16[4,385,256]{2,1,0:T(8,128)(2,1)} %broadcast_in_dim.94), calls=%async_computation.3 | async-start | bytes 1605632 | tf_op jit(solution)/shard_map/all_to_all | solution.py:48
  209.7 30.8 %all-to-all-start.5 = ((bf16[16,128,128]{1,2,0:T(8,128)(2,1)}), bf16[16,128,128]{1,2,0:T(8,128)(2,1)}, u32[]{:S(2)}, u32[]{:S(2)}) async-start(bf16[16,128,128]{1,2,0:T(8,128)(2,1)} %broadcast_in_dim.105), calls=%async_computation.5 | async-start | bytes 1048576 | tf_op jit(solution)/shard_map/all_to_all | solution.py:48
  222.9 17.6 %copy-start.15 = (f32[1,128]{1,0:T(1,128)S(1)}, f32[1,128]{1,0:T(1,128)}, u32[]{:S(2)}) copy-start(f32[1,128]{1,0:T(1,128)} %param.21) | copy-start | bytes 1540
  227.8 0.7 copy-start.7
  243.0 30.9 %copy-start.14 = (bf16[2048,384]{1,0:T(8,128)(2,1)S(1)}, bf16[2048,384]{1,0:T(8,128)(2,1)}, u32[]{:S(2)}) copy-start(bf16[2048,384]{1,0:T(8,128)(2,1)} %all-gather.5.cloned.1.call-done) | copy-start | bytes 4718596
  273.9 0.7 copy-start.13
  274.6 0.7 copy-start.5
  301.8 1.1 copy-start.3
  303.0 4.5 %copy-start.2 = (bf16[768,16,128]{0,2,1:T(8,128)(2,1)S(1)}, bf16[768,16,128]{0,2,1:T(8,128)(2,1)}, u32[]{:S(2)}) copy-start(bf16[768,16,128]{0,2,1:T(8,128)(2,1)} %copy.44) | copy-start | bytes 9437188
  316.0 23.8 %copy-start.6 = (bf16[384,256]{1,0:T(8,128)(2,1)S(1)}, bf16[384,256]{1,0:T(8,128)(2,1)}, u32[]{:S(2)}) copy-start(bf16[384,256]{1,0:T(8,128)(2,1)} %copy-done.5) | copy-start | bytes 589828
Sparse Core Ops, SparseCore 0:
  9.1 125.9 all-gather.2
  167.3 58.7 all-gather.4
